TPU v7x, 32 devices: a whole 2x2x4 slice. The times are simulated.
32 devices in a mesh: grp: 2 (over y), ep: 4 (over z), tp: 4 (over x, core).
Axes of the slice: x: 2, y: 2, z: 4, core: 2. Of those that a mesh axis runs over, the one named last changes fastest.
Arguments:
- query: bfloat16 [8192, 1024], P(('grp', 'ep'), 'tp'), parts along dimension 0, may hold values from -6 to 6
- forget_gate_logits: bfloat16 [8192, 1024], P(('grp', 'ep'), 'tp'), parts along dimension 0, may hold values from -8 to 8
- value: bfloat16 [8192, 1024], P(('grp', 'ep'), 'tp'), parts along dimension 0, may hold values from -6 to 6
- forget_lower_margin: float32 [2, 1024], P(None, 'tp'), may hold values from -30 to -2
- position_log_decay: float32 [8, 8192], P('tp', ('grp', 'ep')), parts along dimension 1, may hold values from -1.5 to 0
- head_norm_gain: float32 [128], replicated, may hold values from 0.1 to 1.9
- mixer_output_weight: bfloat16 [1024, 2048], P('tp'), may hold values from -0.1875 to 0.1875
- second_batch_tokens: bfloat16 [4096, 2048], P(('grp', 'ep', 'tp')), parts along dimension 0, may hold values from -60 to 60
- expert_norm_gain: float32 [2048], replicated, may hold values from 0.1 to 1.9
- routes: int32 [4096, 2], P(('grp', 'ep', 'tp')), parts along dimension 0, may hold values from 0 to 3, all different within a row; in each aligned block of 128 rows (0 to 127, 128 to 255, ...) at most 96 rows name the same one
- chosen_expert_weight: float32 [4096, 2], P(('grp', 'ep', 'tp')), parts along dimension 0, may hold values from 0.2 to 1
- gate_weight: bfloat16 [4, 2048, 2048], P('ep', None, 'tp'), may hold values from -0.3125 to 0.3125
- up_weight: bfloat16 [4, 2048, 2048], P('ep', None, 'tp'), may hold values from -0.3125 to 0.3125
- down_weight: bfloat16 [4, 2048, 2048], P('ep', 'tp'), may hold values from -0.02734375 to 0.02734375
Outputs:
- first_mixer_output: bfloat16 [8192, 2048], P(('grp', 'ep', 'tp')), parts along dimension 0
- moe_out: bfloat16 [4096, 2048], P(('grp', 'ep', 'tp')), parts along dimension 0
There are 2 independent parts, one for each index of `grp`. A program takes and returns all parts, laid end to end along the dimension named above; an argument that names none is the same for every part. Nothing has to cross between parts.
Inputs may be any that keep to these rules, and one draw needn't show every extreme that they name: `routes`: each row names 2 different experts. Among the rows of one device no expert is named by more than 96 rows, and in every draw some expert is named by exactly 96 rows of some device.
All inputs are finite; a program needn't handle non-finite values.
Results may differ from a plain program's by a relative error of at most 0.015.
Values may be sent and summed in bfloat16 or wider, within the bound.
A program may use at most 128 MiB of HBM per device.

v0:
```python
import jax
import jax.numpy as jnp
from jax import lax
from jax.sharding import PartitionSpec as P

HEAD_CHANNELS = 128
BLK = 128
NORM_EPS = 1e-06
CLAMP_LIMIT = 7.0
SIGMOID_SCALE = 1.702
PRECISE = lax.Precision.HIGHEST


def carried_in(value, axis, combine, identity, reverse):
    length, position = (lax.axis_size(axis), lax.axis_index(axis))
    everything = jax.tree.map(
        lambda part, kind: lax.all_gather(part.astype(kind), axis),
        value,
        (jnp.bfloat16, jnp.bfloat16),
    )
    start = jax.tree.map(
        lambda part, zero: jnp.broadcast_to(jnp.asarray(zero, part.dtype), part.shape),
        value,
        identity,
    )

    def turn(k, before):
        at = length - 1 - k if reverse else k
        reached = at > position if reverse else at < position
        new = combine(
            before, jax.tree.map(lambda part, own: part[at].astype(own.dtype), everything, value)
        )
        return jax.tree.map(lambda a, b: jnp.where(reached, a, b), new, before)

    return lax.fori_loop(0, length, turn, start)


def clamped_unit(gate_pre, up_pre):
    gate_pre = jnp.minimum(gate_pre, CLAMP_LIMIT)
    up_pre = jnp.clip(up_pre, -CLAMP_LIMIT, CLAMP_LIMIT)
    return (up_pre + 1.0) * gate_pre * jax.nn.sigmoid(SIGMOID_SCALE * gate_pre)


def local_recurrence(queries, ending_state, values, forget_log_rates):
    sequence_length, number_of_heads, channels = queries.shape
    nblocks = sequence_length // BLK

    def to_blocks(array):
        return array.reshape(nblocks, BLK, number_of_heads, array.shape[-1])

    query_blocks = to_blocks(queries)
    key_blocks = to_blocks(ending_state)
    value_blocks = to_blocks(values)
    cumul = jnp.cumsum(to_blocks(forget_log_rates), axis=1)
    block_last = cumul[:, -1]
    query_in = query_blocks * jnp.exp(cumul)
    key_in = key_blocks * jnp.exp(-cumul)
    key_state = key_blocks * jnp.exp(block_last[:, None] - cumul)
    lower = jnp.tril(jnp.ones((BLK, BLK), jnp.float32))
    scores = jnp.einsum("nchd,nshd->nhcs", query_in, key_in, precision=PRECISE) * lower
    inner = jnp.einsum("nhcs,nshv->nchv", scores, value_blocks, precision=PRECISE)
    increments = jnp.einsum("nshd,nshv->nhdv", key_state, value_blocks, precision=PRECISE)

    def advance(state, inputs):
        decay, increment = inputs
        return (state * decay[..., None] + increment, state)

    initial = jnp.zeros((number_of_heads, channels, values.shape[-1]), jnp.float32)
    final_state, before = lax.scan(advance, initial, (jnp.exp(block_last), increments))
    outer = jnp.einsum("nchd,nhdv->nchv", query_in, before, precision=PRECISE)
    output = (inner + outer).reshape(sequence_length, number_of_heads, values.shape[-1])
    offsets = jnp.cumsum(block_last, axis=0) - block_last
    carried_query = (query_blocks * jnp.exp(cumul + offsets[:, None])).reshape(
        sequence_length, number_of_heads, channels
    )
    total_log = jnp.sum(block_last, axis=0)
    return (output, final_state, total_log, carried_query)


def chain_combine(earlier, later):
    return (earlier[0] * later[0], earlier[1] * later[0][..., None] + later[1])


def mixer_head_states(
    query, forget_gate_logits, value, forget_lower_margin, position_log_decay, head_norm_gain
):
    sequence_length = query.shape[0]
    number_of_heads = query.shape[1] // HEAD_CHANNELS
    queries = jax.nn.silu(query.astype(jnp.float32)).reshape(
        sequence_length, number_of_heads, HEAD_CHANNELS
    ) * HEAD_CHANNELS ** (-0.5)
    values = value.astype(jnp.float32).reshape(sequence_length, number_of_heads, HEAD_CHANNELS)
    shutting = jax.nn.sigmoid(-forget_gate_logits.astype(jnp.float32))
    decay_spikes = jnp.transpose(position_log_decay)[:, :, None]
    ending_state = jnp.exp(forget_lower_margin[0])[None, :] * shutting
    forget_log_rates = (
        jnp.log1p(-ending_state).reshape(sequence_length, number_of_heads, HEAD_CHANNELS)
        + decay_spikes
    )
    ending_state = ending_state.reshape(sequence_length, number_of_heads, HEAD_CHANNELS)
    output, final_state, total_log, carried = local_recurrence(
        queries, ending_state, values, forget_log_rates
    )
    identity = (jnp.ones_like(total_log), jnp.zeros_like(final_state))
    entering = carried_in((jnp.exp(total_log), final_state), "ep", chain_combine, identity, False)[
        1
    ]
    forward = output + jnp.einsum("lhd,hdv->lhv", carried, entering, precision=PRECISE)
    ending_state = jnp.exp(forget_lower_margin[1])[None, :] * shutting
    forget_log_rates = (
        jnp.log1p(-ending_state).reshape(sequence_length, number_of_heads, HEAD_CHANNELS)
        + decay_spikes
    )
    ending_state = ending_state.reshape(sequence_length, number_of_heads, HEAD_CHANNELS)
    output, final_state, total_log, carried = local_recurrence(
        jnp.flip(queries, 0),
        jnp.flip(ending_state, 0),
        jnp.flip(values, 0),
        jnp.flip(forget_log_rates, 0),
    )
    entering = carried_in((jnp.exp(total_log), final_state), "ep", chain_combine, identity, True)[1]
    backward = jnp.flip(
        output + jnp.einsum("lhd,hdv->lhv", carried, entering, precision=PRECISE), 0
    )
    mix = forward + backward
    scaled = (
        mix * lax.rsqrt(jnp.mean(mix * mix, axis=-1, keepdims=True) + NORM_EPS) * head_norm_gain
    )
    return scaled.reshape(sequence_length, number_of_heads * HEAD_CHANNELS).astype(jnp.bfloat16)


def body(
    query,
    forget_gate_logits,
    value,
    forget_lower_margin,
    position_log_decay,
    head_norm_gain,
    mixer_output_weight,
    second_batch_tokens,
    expert_norm_gain,
    routes,
    chosen_expert_weight,
    gate_weight,
    up_weight,
    down_weight,
):
    head_outputs = mixer_head_states(
        query, forget_gate_logits, value, forget_lower_margin, position_log_decay, head_norm_gain
    )
    tokens, top_count = routes.shape
    features = second_batch_tokens.shape[1]
    n_ep = lax.axis_size("ep")
    n_tp = lax.axis_size("tp")
    capacity = (3 * tokens * top_count + 2 * n_ep - 1) // (2 * n_ep)
    tokens_f = second_batch_tokens.astype(jnp.float32)
    normed = (
        tokens_f
        * lax.rsqrt(jnp.mean(tokens_f * tokens_f, axis=-1, keepdims=True) + NORM_EPS)
        * expert_norm_gain
    ).astype(jnp.bfloat16)
    flat_routes = routes.reshape(-1)
    onehot = (flat_routes[:, None] == jnp.arange(n_ep, dtype=jnp.int32)[None, :]).astype(jnp.int32)
    ranking = jnp.cumsum(onehot, axis=0) - onehot
    slot_index = jnp.sum(ranking * onehot, axis=1)
    destination = flat_routes * capacity + slot_index
    source = (
        jnp.full((n_ep * capacity,), tokens, jnp.int32)
        .at[destination]
        .set(jnp.arange(tokens * top_count, dtype=jnp.int32) // top_count)
    )
    padded = jnp.concatenate([normed, jnp.zeros((1, features), jnp.bfloat16)], axis=0)
    send = padded[source]
    expert_block = n_ep * capacity
    copies = jnp.broadcast_to(
        send.reshape(n_ep, 1, capacity, features), (n_ep, n_tp, capacity, features)
    ).reshape(n_ep * n_tp * capacity, features)
    arrived = lax.all_to_all(copies, ("ep", "tp"), split_axis=0, concat_axis=0, tiled=True)
    gate_pre = jnp.dot(arrived, gate_weight[0], preferred_element_type=jnp.float32)
    up_pre = jnp.dot(arrived, up_weight[0], preferred_element_type=jnp.float32)
    hidden = clamped_unit(gate_pre, up_pre).astype(jnp.bfloat16)
    picked = head_outputs
    first_mixer_output = lax.psum_scatter(
        jnp.dot(picked, mixer_output_weight, preferred_element_type=jnp.float32).astype(
            jnp.bfloat16
        ),
        "tp",
        scatter_dimension=0,
        tiled=True,
    )
    block_count = expert_block * lax.axis_size("tp") // expert_block
    grid_view = hidden.reshape(n_ep, n_tp, capacity, hidden.shape[-1])
    picked = grid_view
    picked = jnp.moveaxis(picked, 1, 0).reshape(block_count * expert_block, hidden.shape[-1])
    expert_sum = lax.psum_scatter(
        jnp.dot(picked, down_weight[0], preferred_element_type=jnp.float32).astype(jnp.bfloat16),
        "tp",
        scatter_dimension=0,
        tiled=True,
    )
    returned = lax.all_to_all(expert_sum, "ep", split_axis=0, concat_axis=0, tiled=True)
    gathered = returned[destination].reshape(tokens, top_count, features)
    moe_out = jnp.sum(
        chosen_expert_weight[:, :, None] * gathered.astype(jnp.float32), axis=1
    ).astype(jnp.bfloat16)
    return (first_mixer_output, moe_out)


def solution(mesh):
    return jax.shard_map(
        body,
        mesh=mesh,
        in_specs=(
            P(("grp", "ep"), "tp"),
            P(("grp", "ep"), "tp"),
            P(("grp", "ep"), "tp"),
            P(None, "tp"),
            P("tp", ("grp", "ep")),
            P(),
            P("tp", None),
            P(("grp", "ep", "tp"), None),
            P(),
            P(("grp", "ep", "tp"), None),
            P(("grp", "ep", "tp"), None),
            P("ep", None, "tp"),
            P("ep", None, "tp"),
            P("ep", "tp", None),
        ),
        out_specs=(P(("grp", "ep", "tp"), None), P(("grp", "ep", "tp"), None)),
        check_vma=False,
    )
```

profile of v0, /device:TPU:0, one launch (start us, length us, event | category | flops | bytes accessed | tf_op | source)
XLA Modules:
  0.0 379.8 jit_solution(997884726654975377)
XLA Ops:
  15.0 3.1 gather_fusion
  18.0 4.9 %broadcast_in_dim.32 = bf16[4,4,96,2048]{3,2,1,0:T(8,128)(2,1)} broadcast(bf16[4,96,2048]{2,1,0:T(8,128)(2,1)} %bitcast.183), dimensions={0,2,3} | broadcast | bytes 7864320 | tf_op jit(solution)/shard_map/broadcast_in_dim | solution.py:175
  22.9 7.6 %all-to-all-start = ((bf16[16,96,2048]{2,1,0:T(8,128)(2,1)}), bf16[16,96,2048]{2,1,0:T(8,128)(2,1)}, u32[]{:S(2)}, u32[]{:S(2)}) async-start(bf16[16,96,2048]{2,1,0:T(8,128)(2,1)} %bitcast.178), calls=%async_computation.1 | async-start | bytes 12582912 | tf_op jit(solution)/shard_map/all_to_all | solution.py:178
  31.1 2.3 log-plus-one_bitcast_fusion
  35.2 1.6 fusion.31
  36.8 2.8 copy.175
  39.6 2.5 copy.123
  42.1 2.0 copy.118
  44.2 2.4 multiply_bitcast_fusion
  47.8 2.6 copy.122
  50.4 2.0 reshape_reshape.7
  52.4 3.4 exponential_multiply_fusion.2
  55.9 2.4 convolution_multiply_fusion.1
  58.3 1.6 convolution_bitcast_fusion.5
  59.9 2.0 fusion.25
  63.0 14.2 %while.56 = (s32[]{:T(128)}, f32[2,128,128]{2,1,0:T(8,128)S(1)}, f32[8,2,128,128]{3,2,1,0:T(8,128)}, f32[8,2,128]{2,0,1:T(8,128)S(1)}, f32[8,2,128,128]{3,2,1,0:T(8,128)}, /*index=5*/s32[]{:T(128)}, s32[]{:T(128)}) while((s32[]{:T(128)}, f32[2,128,128]{2,1,0:T(8,128)S(1)}, f32[8,2,128,128]{3,2,1,0:T(8,128)}, ...), condition=%wide.region_2.3_spmd.clone, body=%wide.region_1.2_spmd.clone.sunk | while | flops 131075 | bytes 659040 | solution.py:69
  77.2 67.3 %all-to-all-done = bf16[16,96,2048]{2,1,0:T(8,128)(2,1)} async-done(((bf16[16,96,2048]{2,1,0:T(8,128)(2,1)}), bf16[16,96,2048]{2,1,0:T(8,128)(2,1)}, u32[]{:S(2)}, u32[]{:S(2)}) %all-to-all-start) | async-done | bytes 6291488 | tf_op jit(solution)/shard_map/all_to_all | solution.py:178
  144.6 6.3 %convolution_minimum_fusion = f32[1536,512]{1,0:T(8,128)S(1)} fusion(bf16[1536,2048]{1,0:T(8,128)(2,1)} %bitcast.35, bf16[1,2048,512]{2,1,0:T(8,128)(2,1)} %param.33), kind=kOutput, calls=%fused_computation.18 | convolution fusion | flops 3222011904 | bytes 11534336 | tf_op jit(solution)/shard_map/dot_general | solution.py:179
  150.9 6.9 %fusion.5 = bf16[1536,512]{1,0:T(8,128)(2,1)S(1)} fusion(f32[1536,512]{1,0:T(8,128)S(1)} %convolution_minimum_fusion, bf16[1536,2048]{1,0:T(8,128)(2,1)} %bitcast.35, bf16[1,2048,512]{2,1,0:T(8,128)(2,1)S(1)} %copy-done.22), kind=kOutput, calls=%fused_computation.22 | convolution fusion | flops 3228303360 | bytes 13107200 | tf_op jit(solution)/shard_map/dot_general | solution.py:180
  157.9 5.4 %convolution_convert_fusion = bf16[1536,2048]{1,0:T(8,128)(2,1)} fusion(bf16[1536,512]{1,0:T(8,128)(2,1)S(1)} %bitcast.199, bf16[1,512,2048]{2,1,0:T(8,128)(2,1)S(1)} %copy-done), kind=kOutput, calls=%fused_computation.15 | convolution fusion | flops 3224371200 | bytes 9961472 | tf_op jit(solution)/shard_map/dot_general | solution.py:196
  164.9 2.1 fusion.13
  171.2 1.7 rev.17
  174.1 1.9 fusion.23
  177.0 7.5 %rev.18 = f32[1024,2,128]{0,2,1:T(8,128)S(1)} reverse(f32[1024,2,128]{0,2,1:T(8,128)} %bitcast.193), dimensions={0} | reverse | bytes 2097152 | tf_op jit(solution)/shard_map/jit(_flip)/rev | solution.py:117
  188.8 5.9 %rev.19 = f32[1024,2,128]{0,2,1:T(8,128)} reverse(bf16[1024,2,128]{0,2,1:T(8,128)(2,1)S(1)} %bitcast.196), dimensions={0} | reverse | bytes 1572864 | tf_op jit(solution)/shard_map/jit(_flip)/rev | solution.py:118
  194.8 1.9 copy.147
  198.2 4.5 %exponential_multiply_fusion = (f32[8,128,2,128]{3,0,1,2:T(8,128)S(1)}, f32[8,128,2,128]{3,0,1,2:T(8,128)S(1)}, f32[8,128,2,128]{3,0,1,2:T(8,128)}, f32[8,128,2,128]{3,0,1,2:T(8,128)S(1)}) fusion(f32[8,128,2,128]{3,0,1,2:T(8,128)} %copy-done.8, f32[8,128,2,128]{3,1,0,2:T(8,128)} %bitcast.184, f32[8,2,128]{2,0,1:T(8,128)S(1)} %get-tuple-element.453, ...), kind=kLoop, calls=%fused_computation.63 | loop fusion | flops 1572864 | bytes 7356416 | tf_op jit(solution)/shard_map/mul | solution.py:58
  202.7 2.4 convolution_multiply_fusion
  205.1 2.2 convolution_bitcast_fusion.2
  207.3 2.9 fusion.20
  211.3 13.7 %while.58 = (s32[]{:T(128)}, f32[2,128,128]{2,1,0:T(8,128)S(1)}, f32[8,2,128,128]{3,2,1,0:T(8,128)}, f32[8,2,128]{2,0,1:T(8,128)S(1)}, f32[8,2,128,128]{3,2,1,0:T(8,128)}, /*index=5*/s32[]{:T(128)}, s32[]{:T(128)}) while((s32[]{:T(128)}, f32[2,128,128]{2,1,0:T(8,128)S(1)}, f32[8,2,128,128]{3,2,1,0:T(8,128)}, ...), condition=%wide.region_9.10_spmd.clone, body=%wide.region_8.9_spmd.clone.sunk | while | flops 131075 | bytes 659040 | solution.py:69
  225.0 3.4 fusion.10
  228.4 1.8 copy.154
  232.6 2.5 copy.156
  235.2 31.3 %all-gather.5 = bf16[4,2,128]{2,1,0:T(2,128)(2,1)S(1)} all-gather(bf16[1,2,128]{2,1,0:T(2,128)(2,1)S(1)} %fusion.50), channel_id=4, replica_groups=mesh['grp'=2,'ep'=4,'tp'=4] {'ep'}, dimensions={0}, use_global_device_ids=true | all-gather | bytes 2560 | tf_op jit(solution)/shard_map/all_gather | solution.py:17
  266.4 13.9 %all-gather.3 = bf16[8,128,128]{2,1,0:T(8,128)(2,1)S(1)} all-gather(bf16[2,128,128]{2,1,0:T(8,128)(2,1)S(1)} %convert_element_type.137), channel_id=5, replica_groups=mesh['grp'=2,'ep'=4,'tp'=4] {'ep'}, dimensions={0}, use_global_device_ids=true | all-gather | bytes 327680 | tf_op jit(solution)/shard_map/all_gather | solution.py:17
  281.2 3.6 fusion.9
  284.9 9.4 %rev.20 = f32[1024,2,128]{0,2,1:T(8,128)} reverse(f32[1024,2,128]{0,2,1:T(8,128)} %fusion.9), dimensions={0} | reverse | bytes 2097152 | tf_op jit(solution)/shard_map/jit(_flip)/rev | solution.py:122
  295.5 2.7 copy.134
  298.2 9.7 %all-gather.4 = bf16[4,2,128]{2,1,0:T(2,128)(2,1)S(1)} all-gather(bf16[1,2,128]{2,1,0:T(2,128)(2,1)S(1)} %fusion.49), channel_id=2, replica_groups=mesh['grp'=2,'ep'=4,'tp'=4] {'ep'}, dimensions={0}, use_global_device_ids=true | all-gather | bytes 2560 | tf_op jit(solution)/shard_map/all_gather | solution.py:17
  307.9 13.8 %all-gather.1 = bf16[8,128,128]{2,1,0:T(8,128)(2,1)S(1)} all-gather(bf16[2,128,128]{2,1,0:T(8,128)(2,1)S(1)} %convert_element_type.134), channel_id=3, replica_groups=mesh['grp'=2,'ep'=4,'tp'=4] {'ep'}, dimensions={0}, use_global_device_ids=true | all-gather | bytes 327680 | tf_op jit(solution)/shard_map/all_gather | solution.py:17
  322.4 2.8 multiply_reduce_fusion.1
  325.4 3.3 convolution_convert_fusion.1
  328.7 4.4 %all-to-all-start.1 = ((bf16[4,96,2048]{2,1,0:T(8,128)(2,1)}), bf16[4,96,2048]{2,1,0:T(8,128)(2,1)}, u32[]{:S(2)}, u32[]{:S(2)}) async-start(bf16[4,96,2048]{2,1,0:T(8,128)(2,1)} %bitcast.197), calls=%async_computation.3 | async-start | bytes 3145728 | tf_op jit(solution)/shard_map/all_to_all | solution.py:201
  333.2 27.1 %all-to-all-done.1 = bf16[4,96,2048]{2,1,0:T(8,128)(2,1)} async-done(((bf16[4,96,2048]{2,1,0:T(8,128)(2,1)}), bf16[4,96,2048]{2,1,0:T(8,128)(2,1)}, u32[]{:S(2)}, u32[]{:S(2)}) %all-to-all-start.1) | async-done | bytes 1572896 | tf_op jit(solution)/shard_map/all_to_all | solution.py:201
  360.3 4.1 %gather_fusion.1 = bf16[256,2048]{1,0:T(8,128)(2,1)S(1)} fusion(bf16[384,2048]{1,0:T(8,128)(2,1)} %bitcast.43, s32[1024]{0:T(1024)S(1)} %pad_clamp_fusion), kind=kCustom, calls=%fused_computation.1 | custom fusion | bytes 2098176 | tf_op jit(solution)/shard_map/gather | solution.py:202
  364.5 2.4 reshape.232
  366.8 5.6 %multiply_reduce_fusion = bf16[128,2048]{1,0:T(8,128)(2,1)} fusion(f32[128,2,2048]{2,1,0:T(2,128)} %reshape.232, f32[128,2]{1,0:T(8,128)S(1)} %copy.159), kind=kLoop, calls=%fused_computation.26 | loop fusion | flops 786432 | bytes 2622464 | tf_op jit(solution)/shard_map/reduce_sum | solution.py:203
  (185 shorter events, 61.2 us)
Async XLA Ops:
  7.2 150.8 %copy-start = (bf16[1,512,2048]{2,1,0:T(8,128)(2,1)S(1)}, bf16[1,512,2048]{2,1,0:T(8,128)(2,1)}, u32[]{:S(2)}) copy-start(bf16[1,512,2048]{2,1,0:T(8,128)(2,1)} %param.35) | copy-start | bytes 6291460
  22.9 7.9 %copy-start.17 = (bf16[1024,256]{1,0:T(8,128)(2,1)S(1)}, bf16[1024,256]{1,0:T(8,128)(2,1)}, u32[]{:S(2)}) copy-start(bf16[1024,256]{1,0:T(8,128)(2,1)} %param.23) | copy-start | bytes 1572868
  22.9 8.1 %copy-start.19 = (f32[2,256]{1,0:T(2,128)S(1)}, f32[2,256]{1,0:T(2,128)}, u32[]{:S(2)}) copy-start(f32[2,256]{1,0:T(2,128)} %param.25) | copy-start | bytes 6148
  22.9 121.6 %all-to-all-start = ((bf16[16,96,2048]{2,1,0:T(8,128)(2,1)}), bf16[16,96,2048]{2,1,0:T(8,128)(2,1)}, u32[]{:S(2)}, u32[]{:S(2)}) async-start(bf16[16,96,2048]{2,1,0:T(8,128)(2,1)} %bitcast.178), calls=%async_computation.1 | async-start | bytes 12582912 | tf_op jit(solution)/shard_map/all_to_all | solution.py:178
  30.5 298.2 %reduce-scatter.5.cloned.1.call-start = ((), (), s32[]{:S(2)}) async-start(), calls=%async_computation.5 | async-start | bytes 7864320 | tf_op jit(solution)/shard_map/reduce_scatter | solution.py:195
  33.4 1.6 copy-start.18
  36.8 15.7 %copy-start.7 = (f32[8,128,2,128]{3,0,1,2:T(8,128)}, f32[8,128,2,128]{3,0,1,2:T(8,128)S(1)}, u32[]{:S(2)}) copy-start(f32[8,128,2,128]{3,0,1,2:T(8,128)S(1)} %fusion.31) | copy-start | bytes 3145732
  55.9 2.4 copy-start.6
  144.6 6.3 %copy-start.22 = (bf16[1,2048,512]{2,1,0:T(8,128)(2,1)S(1)}, bf16[1,2048,512]{2,1,0:T(8,128)(2,1)}, u32[]{:S(2)}) copy-start(bf16[1,2048,512]{2,1,0:T(8,128)(2,1)} %param.34) | copy-start | bytes 6291460
  163.3 1.2 copy-start.14
  163.3 1.5 copy-start.15
  163.3 209.4 %reduce-scatter.3.cloned.1.call-start = ((), (), s32[]{:S(2)}) async-start(), calls=%async_computation.4 | async-start | bytes 5242880 | tf_op jit(solution)/shard_map/reduce_scatter | solution.py:183
  167.0 4.0 %copy-start.13 = (f32[1024,256]{0,1:T(8,128)S(1)}, f32[1024,256]{0,1:T(8,128)}, u32[]{:S(2)}) copy-start(f32[1024,256]{0,1:T(8,128)} %get-tuple-element.462) | copy-start | bytes 3145732
  174.1 11.8 %copy-start.2 = (f32[1024,256]{0,1:T(8,128)S(1)}, f32[1024,256]{0,1:T(8,128)}, u32[]{:S(2)}) copy-start(f32[1024,256]{0,1:T(8,128)} %get-tuple-element.461) | copy-start | bytes 3145732
  176.1 1.0 copy-start.8
  187.4 9.2 %copy-start.4 = (f32[1024,2,128]{0,2,1:T(8,128)}, f32[1024,2,128]{0,2,1:T(8,128)S(1)}, u32[]{:S(2)}) copy-start(f32[1024,2,128]{0,2,1:T(8,128)S(1)} %reverse.3) | copy-start | bytes 3145732
  210.2 14.8 %copy-start.11 = (f32[8,128,2,128]{3,1,2,0:T(8,128)S(1)}, f32[8,128,2,128]{3,1,2,0:T(8,128)}, u32[]{:S(2)}) copy-start(f32[8,128,2,128]{3,1,2,0:T(8,128)} %convolution_bitcast_fusion.2) | copy-start | bytes 3145732
  228.4 3.0 copy-start.10
  231.4 49.8 %copy-start.5 = (f32[1024,2,128]{0,2,1:T(8,128)S(1)}, f32[1024,2,128]{0,2,1:T(8,128)}, u32[]{:S(2)}) copy-start(f32[1024,2,128]{0,2,1:T(8,128)} %copy-done.4) | copy-start | bytes 3145732
  281.2 13.0 %copy-start.9 = (f32[8,128,2,128]{3,0,1,2:T(8,128)S(1)}, f32[8,128,2,128]{3,0,1,2:T(8,128)}, u32[]{:S(2)}) copy-start(f32[8,128,2,128]{3,0,1,2:T(8,128)} %get-tuple-element.446) | copy-start | bytes 3145732
  294.3 28.1 %copy-start.3 = (f32[1024,256]{0,1:T(8,128)S(1)}, f32[1024,256]{0,1:T(8,128)}, u32[]{:S(2)}) copy-start(f32[1024,256]{0,1:T(8,128)} %get-tuple-element.461) | copy-start | bytes 3145732
  295.5 26.9 %copy-start.12 = (f32[1024,2,128]{0,2,1:T(8,128)S(1)}, f32[1024,2,128]{0,2,1:T(8,128)}, u32[]{:S(2)}) copy-start(f32[1024,2,128]{0,2,1:T(8,128)} %copy.137) | copy-start | bytes 3145732
  322.4 2.8 copy-start.21
  322.4 3.0 copy-start.16
  328.7 4.4 %copy-start.20 = (f32[128,2]{0,1:T(2,128)S(1)}, f32[128,2]{0,1:T(2,128)}, u32[]{:S(2)}) copy-start(f32[128,2]{0,1:T(2,128)} %param.32) | copy-start | bytes 3076
  328.7 31.6 %all-to-all-start.1 = ((bf16[4,96,2048]{2,1,0:T(8,128)(2,1)}), bf16[4,96,2048]{2,1,0:T(8,128)(2,1)}, u32[]{:S(2)}, u32[]{:S(2)}) async-start(bf16[4,96,2048]{2,1,0:T(8,128)(2,1)} %bitcast.197), calls=%async_computation.3 | async-start | bytes 3145728 | tf_op jit(solution)/shard_map/all_to_all | solution.py:201
  360.3 12.5 %copy-start.1 = (bf16[1,512,2048]{2,1,0:T(8,128)(2,1)S(1)}, bf16[1,512,2048]{2,1,0:T(8,128)(2,1)}, u32[]{:S(2)}) copy-start(bf16[1,512,2048]{2,1,0:T(8,128)(2,1)} %param.35) | copy-start | bytes 6291460
Sparse Core Ops, SparseCore 0:
  163.5 82.2 reduce-scatter.4
  328.8 43.8 reduce-scatter.2
where the time goes:
time: 386 us; the launch traced here: 380 us
  waiting for transfers between devices  94.8 us (25%)
  local copies, waits for them, and re-layouts  84.8 us (22%)
  blocking collectives  68.7 us (18%)
  other arithmetic  55.6 us (14%)
  matrix products  47.5 us (12%)
  between operations  14.8 us (4%)
  starting transfers between devices  12.3 us (3%)
    all_gather x4, blocking collectives, carried_in(): lax.all_gather(part.astype(kind), axis)  68.7 us
    all_to_all x1, waiting for transfers between devices, body(): lax.all_to_all(copies, ('ep', 'tp'), split_axis=0, concat_axis=0, tiled=T...  67.3 us
    all_to_all x1, waiting for transfers between devices, body(): lax.all_to_all(expert_sum, 'ep', split_axis=0, concat_axis=0, tiled=True)  27.1 us
    add x16, other arithmetic, advance(): return (state * decay[..., None] + increment, state)  16.3 us
    unnamed x55, local copies, waits for them, and re-layouts  11.4 us
    dynamic_update_slice x16, other arithmetic, local_recurrence(): lax.scan(advance, initial, (jnp.exp(block_last), increments))  10.6 us
    rev x1, local copies, waits for them, and re-layouts, mixer_head_states(): jnp.flip(output + jnp.einsum('lhd,hdv->lhv', carried, entering, precision...  9.37 us
    rev x2, local copies, waits for them, and re-layouts, mixer_head_states(): jnp.flip(ending_state, 0)  8.89 us
  transfers between devices with their start and end apart: 4, of which 3 were waited for; matrix products, arithmetic and copies ran while one was open for 40% of the time, Pallas kernels for 0%

commit v1 on v0

--- a/solution.py
+++ b/solution.py
@@ -9,6 +9,18 @@
 CLAMP_LIMIT = 7.0
 SIGMOID_SCALE = 1.702
 PRECISE = lax.Precision.HIGHEST
+
+
+def split_up(array, dim, peers):
+    shape = array.shape
+    pieces = array.reshape(*shape[:dim], peers, shape[dim] // peers, *shape[dim + 1 :])
+    return jnp.moveaxis(pieces, dim, 0)
+
+
+def joined_along(parts, dim):
+    lengths = list(parts.shape[1:])
+    lengths[dim] *= parts.shape[0]
+    return jnp.moveaxis(parts, 0, dim).reshape(lengths)
 
 
 def carried_in(value, axis, combine, identity, reverse):
@@ -198,7 +210,15 @@
         scatter_dimension=0,
         tiled=True,
     )
-    returned = lax.all_to_all(expert_sum, "ep", split_axis=0, concat_axis=0, tiled=True)
+    size, index = (lax.axis_size("ep"), lax.axis_index("ep"))
+    parts = split_up(expert_sum, 0, size)
+    filled = parts
+    for lap in range(1, size):
+        target, source_2 = ((index + lap) % size, (index - lap) % size)
+        sent = lax.dynamic_index_in_dim(parts, target, 0)
+        theirs = lax.ppermute(sent, "ep", [(i, (i + lap) % size) for i in range(size)])
+        filled = lax.dynamic_update_slice_in_dim(filled, theirs, source_2, axis=0)
+    returned = joined_along(filled, 0)
     gathered = returned[destination].reshape(tokens, top_count, features)
     moe_out = jnp.sum(
         chosen_expert_weight[:, :, None] * gathered.astype(jnp.float32), axis=1

time: 386 us -> 366 us (0.948)
  waiting for transfers between devices: 94.8 us -> 68.8 us
    all_to_all x1 -> x0, waiting for transfers between devices: 27.1 us -> none  [body(): lax.all_to_all(expert_sum, 'ep', split_axis=0, concat_axis=0, tiled=True)]
    ppermute x0 -> x3, waiting for transfers between devices: none -> 24 us  [body(): lax.ppermute(sent, 'ep', [(i, (i + lap) % size) for i in range(size)])]
    all_to_all x1, waiting for transfers between devices: 67.3 us -> 44.8 us  [body(): lax.all_to_all(copies, ('ep', 'tp'), split_axis=0, concat_axis=0, tiled=T...]
    ppermute x0 -> x3, starting transfers between devices: none -> 6.35 us  [body(): lax.ppermute(sent, 'ep', [(i, (i + lap) % size) for i in range(size)])]
    rev x2, local copies, waits for them, and re-layouts: 2.99 us -> 7.85 us  [mixer_head_states(): jnp.flip(forget_log_rates, 0)]
    another operation x5, local copies, waits for them, and re-layouts: 3.75 us -> 8.47 us
    exp x4, local copies, waits for them, and re-layouts: 7.57 us -> 3.05 us  [local_recurrence(): jnp.exp(cumul + offsets[:, None])]
    all_to_all x1 -> x0, starting transfers between devices: 4.35 us -> none  [body(): lax.all_to_all(expert_sum, 'ep', split_axis=0, concat_axis=0, tiled=True)]
  transfers between devices with their start and end apart: 4 -> 6, of which waited for: 3 -> 4; matrix products, arithmetic and copies ran while one was open for 40% -> 42% of each run, Pallas kernels for 0% -> 0%
where the time goes in v1:
time: 366 us; the launch traced here: 359 us
  local copies, waits for them, and re-layouts  88.4 us (24%)
  blocking collectives  69.1 us (19%)
  waiting for transfers between devices  68.8 us (19%)
  other arithmetic  55.3 us (15%)
  matrix products  47.7 us (13%)
  between operations  14.9 us (4%)
  starting transfers between devices  14 us (4%)
    all_gather x4, blocking collectives, carried_in(): lax.all_gather(part.astype(kind), axis)  69.1 us
    all_to_all x1, waiting for transfers between devices, body(): lax.all_to_all(copies, ('ep', 'tp'), split_axis=0, concat_axis=0, tiled=T...  44.8 us
    ppermute x3, waiting for transfers between devices, body(): lax.ppermute(sent, 'ep', [(i, (i + lap) % size) for i in range(size)])  24 us
    add x16, other arithmetic, advance(): return (state * decay[..., None] + increment, state)  16.3 us
    unnamed x53, local copies, waits for them, and re-layouts  11.1 us
    dynamic_update_slice x16, other arithmetic, local_recurrence(): lax.scan(advance, initial, (jnp.exp(block_last), increments))  10.7 us
    rev x2, local copies, waits for them, and re-layouts, mixer_head_states(): jnp.flip(ending_state, 0)  8.82 us
    another operation x5, local copies, waits for them, and re-layouts  8.47 us
  transfers between devices with their start and end apart: 6, of which 4 were waited for; matrix products, arithmetic and copies ran while one was open for 42% of the time, Pallas kernels for 0%

profile of v1, /device:TPU:0, one launch (start us, length us, event | category | flops | bytes accessed | tf_op | source)
XLA Modules:
  0.0 359.4 jit_solution(4689369173254179662)
XLA Ops:
  11.0 1.4 scatter_custom_fusion
  15.0 3.1 gather_fusion
  18.0 4.9 %broadcast_in_dim.32 = bf16[4,4,96,2048]{3,2,1,0:T(8,128)(2,1)} broadcast(bf16[4,96,2048]{2,1,0:T(8,128)(2,1)} %bitcast.186), dimensions={0,2,3} | broadcast | bytes 7864320 | tf_op jit(solution)/shard_map/broadcast_in_dim | solution.py:187
  22.9 7.6 %all-to-all-start = ((bf16[16,96,2048]{2,1,0:T(8,128)(2,1)}), bf16[16,96,2048]{2,1,0:T(8,128)(2,1)}, u32[]{:S(2)}, u32[]{:S(2)}) async-start(bf16[16,96,2048]{2,1,0:T(8,128)(2,1)} %bitcast.181), calls=%async_computation.1 | async-start | bytes 12582912 | tf_op jit(solution)/shard_map/all_to_all | solution.py:190
  30.8 2.4 log-plus-one_bitcast_fusion
  33.3 6.3 %rev.17 = f32[1024,2,128]{0,2,1:T(8,128)} reverse(f32[1024,2,128]{0,2,1:T(8,128)S(1)} %broadcast_add_fusion), dimensions={0} | reverse | bytes 2097152 | tf_op jit(solution)/shard_map/jit(_flip)/rev | solution.py:131
  39.6 1.5 copy.139
  42.8 7.5 %rev.18 = f32[1024,2,128]{0,2,1:T(8,128)S(1)} reverse(f32[1024,2,128]{0,2,1:T(8,128)} %bitcast.196), dimensions={0} | reverse | bytes 2097152 | tf_op jit(solution)/shard_map/jit(_flip)/rev | solution.py:129
  51.6 2.0 copy.118
  53.7 2.4 multiply_bitcast_fusion
  56.1 6.1 %reverse.3 = f32[1024,2,128]{0,2,1:T(8,128)} reverse(f32[1024,2,128]{0,2,1:T(8,128)S(1)} %bitcast.184), dimensions={0} | reverse | bytes 2097152 | tf_op jit(solution)/shard_map/reverse
  62.2 2.3 broadcast_multiply_fusion.1
  64.5 2.6 copy.138
  68.4 5.9 %rev.19 = f32[1024,2,128]{0,2,1:T(8,128)} reverse(bf16[1024,2,128]{0,2,1:T(8,128)(2,1)S(1)} %bitcast.199), dimensions={0} | reverse | bytes 1572864 | tf_op jit(solution)/shard_map/jit(_flip)/rev | solution.py:130
  74.3 1.5 copy.147
  77.3 4.7 %exponential_multiply_fusion = (f32[8,128,2,128]{3,0,1,2:T(8,128)S(1)}, f32[8,128,2,128]{3,0,1,2:T(8,128)}, f32[8,128,2,128]{3,0,1,2:T(8,128)}, f32[8,128,2,128]{3,0,1,2:T(8,128)}) fusion(f32[8,128,2,128]{3,0,1,2:T(8,128)} %copy-done.6, f32[8,128,2,128]{3,1,0,2:T(8,128)} %bitcast.187, f32[8,2,128]{2,0,1:T(8,128)S(1)} %get-tuple-element.456, ...), kind=kLoop, calls=%fused_computation.63 | loop fusion | flops 1572864 | bytes 7356416 | tf_op jit(solution)/shard_map/mul | solution.py:70
  82.0 2.9 fusion.20
  86.0 13.7 %while.58 = (s32[]{:T(128)}, f32[2,128,128]{2,1,0:T(8,128)S(1)}, f32[8,2,128,128]{3,2,1,0:T(8,128)}, f32[8,2,128]{2,0,1:T(8,128)S(1)}, f32[8,2,128,128]{3,2,1,0:T(8,128)}, /*index=5*/s32[]{:T(128)}, s32[]{:T(128)}) while((s32[]{:T(128)}, f32[2,128,128]{2,1,0:T(8,128)S(1)}, f32[8,2,128,128]{3,2,1,0:T(8,128)}, ...), condition=%wide.region_9.10_spmd.clone, body=%wide.region_8.9_spmd.clone.sunk | while | flops 131075 | bytes 659040 | solution.py:81
  99.7 44.8 %all-to-all-done = bf16[16,96,2048]{2,1,0:T(8,128)(2,1)} async-done(((bf16[16,96,2048]{2,1,0:T(8,128)(2,1)}), bf16[16,96,2048]{2,1,0:T(8,128)(2,1)}, u32[]{:S(2)}, u32[]{:S(2)}) %all-to-all-start) | async-done | bytes 6291488 | tf_op jit(solution)/shard_map/all_to_all | solution.py:190
  144.6 6.3 %convolution_minimum_fusion = f32[1536,512]{1,0:T(8,128)S(1)} fusion(bf16[1536,2048]{1,0:T(8,128)(2,1)} %bitcast.35, bf16[1,2048,512]{2,1,0:T(8,128)(2,1)} %param.33), kind=kOutput, calls=%fused_computation.18 | convolution fusion | flops 3222011904 | bytes 11534336 | tf_op jit(solution)/shard_map/dot_general | solution.py:191
  150.9 6.9 %fusion.5 = bf16[1536,512]{1,0:T(8,128)(2,1)S(1)} fusion(f32[1536,512]{1,0:T(8,128)S(1)} %convolution_minimum_fusion, bf16[1536,2048]{1,0:T(8,128)(2,1)} %bitcast.35, bf16[1,2048,512]{2,1,0:T(8,128)(2,1)S(1)} %copy-done.21), kind=kOutput, calls=%fused_computation.22 | convolution fusion | flops 3228303360 | bytes 13107200 | tf_op jit(solution)/shard_map/dot_general | solution.py:192
  157.9 5.9 %convolution_convert_fusion = bf16[1536,2048]{1,0:T(8,128)(2,1)} fusion(bf16[1536,512]{1,0:T(8,128)(2,1)S(1)} %bitcast.201, bf16[1,512,2048]{2,1,0:T(8,128)(2,1)S(1)} %copy-done), kind=kOutput, calls=%fused_computation.15 | convolution fusion | flops 3224371200 | bytes 9961472 | tf_op jit(solution)/shard_map/dot_general | solution.py:208
  165.1 4.6 %convolution_multiply_fusion = f32[8,2,128,128]{3,2,1,0:T(8,128)} fusion(f32[8,128,2,128]{3,0,1,2:T(8,128)} %get-tuple-element.445, f32[8,128,2,128]{3,0,1,2:T(8,128)S(1)} %copy-done.2, f32[128,128]{1,0:T(8,128)S(1)} %fusion.43), kind=kOutput, calls=%fused_computation.32 | convolution fusion | flops 402915328 | bytes 3211264 | tf_op jit(solution)/shard_map/nchd,nshd->nhcs/dot_general | solution.py:72
  170.9 2.5 convolution_bitcast_fusion.2
  173.4 2.2 fusion.10
  175.6 1.7 copy.154
  180.0 31.6 %all-gather.5 = bf16[4,2,128]{2,1,0:T(2,128)(2,1)S(1)} all-gather(bf16[1,2,128]{2,1,0:T(2,128)(2,1)S(1)} %fusion.50), channel_id=4, replica_groups=mesh['grp'=2,'ep'=4,'tp'=4] {'ep'}, dimensions={0}, use_global_device_ids=true | all-gather | bytes 2560 | tf_op jit(solution)/shard_map/all_gather | solution.py:29
  211.6 14.0 %all-gather.3 = bf16[8,128,128]{2,1,0:T(8,128)(2,1)S(1)} all-gather(bf16[2,128,128]{2,1,0:T(8,128)(2,1)S(1)} %convert_element_type.137), channel_id=5, replica_groups=mesh['grp'=2,'ep'=4,'tp'=4] {'ep'}, dimensions={0}, use_global_device_ids=true | all-gather | bytes 327680 | tf_op jit(solution)/shard_map/all_gather | solution.py:29
  226.6 2.6 fusion.9
  229.2 6.0 %rev.20 = f32[1024,2,128]{0,2,1:T(8,128)} reverse(f32[1024,2,128]{0,2,1:T(8,128)S(1)} %fusion.9), dimensions={0} | reverse | bytes 2097152 | tf_op jit(solution)/shard_map/jit(_flip)/rev | solution.py:134
  238.3 2.5 copy.123
  242.0 2.6 copy.122
  244.7 3.1 exponential_multiply_fusion.2
  247.8 2.4 convolution_multiply_fusion.1
  250.9 2.0 fusion.25
  254.1 13.7 %while.56 = (s32[]{:T(128)}, f32[2,128,128]{2,1,0:T(8,128)S(1)}, f32[8,2,128,128]{3,2,1,0:T(8,128)}, f32[8,2,128]{2,0,1:T(8,128)S(1)}, f32[8,2,128,128]{3,2,1,0:T(8,128)}, /*index=5*/s32[]{:T(128)}, s32[]{:T(128)}) while((s32[]{:T(128)}, f32[2,128,128]{2,1,0:T(8,128)S(1)}, f32[8,2,128,128]{3,2,1,0:T(8,128)}, ...), condition=%wide.region_2.3_spmd.clone, body=%wide.region_1.2_spmd.clone.sunk | while | flops 131075 | bytes 659040 | solution.py:81
  267.8 2.4 fusion.13
  273.3 9.7 %all-gather.4 = bf16[4,2,128]{2,1,0:T(2,128)(2,1)S(1)} all-gather(bf16[1,2,128]{2,1,0:T(2,128)(2,1)S(1)} %fusion.49), channel_id=2, replica_groups=mesh['grp'=2,'ep'=4,'tp'=4] {'ep'}, dimensions={0}, use_global_device_ids=true | all-gather | bytes 2560 | tf_op jit(solution)/shard_map/all_gather | solution.py:29
  283.0 13.8 %all-gather.1 = bf16[8,128,128]{2,1,0:T(8,128)(2,1)S(1)} all-gather(bf16[2,128,128]{2,1,0:T(8,128)(2,1)S(1)} %convert_element_type.134), channel_id=3, replica_groups=mesh['grp'=2,'ep'=4,'tp'=4] {'ep'}, dimensions={0}, use_global_device_ids=true | all-gather | bytes 327680 | tf_op jit(solution)/shard_map/all_gather | solution.py:29
  297.7 3.0 multiply_reduce_fusion.1
  301.9 3.3 convolution_convert_fusion.1
  306.4 13.8 %collective-permute-done = bf16[1,96,2048]{2,1,0:T(8,128)(2,1)S(1)} collective-permute-done((bf16[1,96,2048]{2,1,0:T(8,128)(2,1)S(1)}, bf16[1,96,2048]{2,1,0:T(8,128)(2,1)S(1)}, u32[]{:S(2)}, u32[]{:S(2)}) %collective-permute-start) | collective-permute-done | bytes 393248 | tf_op jit(solution)/shard_map/ppermute | solution.py:219
  320.2 2.0 constant_dynamic-slice_fusion.2
  322.2 5.9 %collective-permute-start.1 = (bf16[1,96,2048]{2,1,0:T(8,128)(2,1)S(1)}, bf16[1,96,2048]{2,1,0:T(8,128)(2,1)S(1)}, u32[]{:S(2)}, u32[]{:S(2)}) collective-permute-start(bf16[1,96,2048]{2,1,0:T(8,128)(2,1)S(1)} %get-tuple-element.447), channel_id=1, source_target_pairs={{0,8},{4,12},{8,0},{12,4},{1,9},{5,13},{9,1},{13,5},{2,10},{6,14},... | collective-permute-start | bytes 1179656 | tf_op jit(solution)/shard_map/ppermute | solution.py:219
  328.7 9.5 %collective-permute-done.1 = bf16[1,96,2048]{2,1,0:T(8,128)(2,1)S(1)} collective-permute-done((bf16[1,96,2048]{2,1,0:T(8,128)(2,1)S(1)}, bf16[1,96,2048]{2,1,0:T(8,128)(2,1)S(1)}, u32[]{:S(2)}, u32[]{:S(2)}) %collective-permute-start.1) | collective-permute-done | bytes 393248 | tf_op jit(solution)/shard_map/ppermute | solution.py:219
  340.4 4.0 %gather_fusion.1 = bf16[256,2048]{1,0:T(8,128)(2,1)S(1)} fusion(bf16[384,2048]{1,0:T(8,128)(2,1)} %bitcast.180, s32[1024]{0:T(1024)S(1)} %pad_clamp_fusion), kind=kCustom, calls=%fused_computation.1 | custom fusion | bytes 2098176 | tf_op jit(solution)/shard_map/gather | solution.py:222
  344.4 2.3 reshape.238
  346.7 5.6 %multiply_reduce_fusion = bf16[128,2048]{1,0:T(8,128)(2,1)} fusion(f32[128,2,2048]{2,1,0:T(2,128)} %reshape.238, f32[128,2]{1,0:T(8,128)S(1)} %copy.159), kind=kLoop, calls=%fused_computation.26 | loop fusion | flops 786432 | bytes 2622464 | tf_op jit(solution)/shard_map/reduce_sum | solution.py:223
  (192 shorter events, 62.9 us)
Async XLA Ops:
  7.2 150.8 %copy-start = (bf16[1,512,2048]{2,1,0:T(8,128)(2,1)S(1)}, bf16[1,512,2048]{2,1,0:T(8,128)(2,1)}, u32[]{:S(2)}) copy-start(bf16[1,512,2048]{2,1,0:T(8,128)(2,1)} %param.35) | copy-start | bytes 6291460
  22.9 7.6 %copy-start.16 = (bf16[1024,256]{1,0:T(8,128)(2,1)S(1)}, bf16[1024,256]{1,0:T(8,128)(2,1)}, u32[]{:S(2)}) copy-start(bf16[1024,256]{1,0:T(8,128)(2,1)} %param.23) | copy-start | bytes 1572868
  22.9 7.9 %copy-start.18 = (f32[2,256]{1,0:T(2,128)S(1)}, f32[2,256]{1,0:T(2,128)}, u32[]{:S(2)}) copy-start(f32[2,256]{1,0:T(2,128)} %param.25) | copy-start | bytes 6148
  22.9 121.6 %all-to-all-start = ((bf16[16,96,2048]{2,1,0:T(8,128)(2,1)}), bf16[16,96,2048]{2,1,0:T(8,128)(2,1)}, u32[]{:S(2)}, u32[]{:S(2)}) async-start(bf16[16,96,2048]{2,1,0:T(8,128)(2,1)} %bitcast.181), calls=%async_computation.1 | async-start | bytes 12582912 | tf_op jit(solution)/shard_map/all_to_all | solution.py:190
  30.5 274.8 %reduce-scatter.5.cloned.1.call-start = ((), (), s32[]{:S(2)}) async-start(), calls=%async_computation.4 | async-start | bytes 7864320 | tf_op jit(solution)/shard_map/reduce_scatter | solution.py:207
  30.8 2.4 copy-start.17
  41.8 1.0 copy-start.6
  56.1 8.5 %copy-start.3 = (f32[1024,256]{0,1:T(8,128)}, f32[1024,256]{0,1:T(8,128)S(1)}, u32[]{:S(2)}) copy-start(f32[1024,256]{0,1:T(8,128)S(1)} %get-tuple-element.464) | copy-start | bytes 3145732
  144.6 6.3 %copy-start.21 = (bf16[1,2048,512]{2,1,0:T(8,128)(2,1)S(1)}, bf16[1,2048,512]{2,1,0:T(8,128)(2,1)}, u32[]{:S(2)}) copy-start(bf16[1,2048,512]{2,1,0:T(8,128)(2,1)} %param.34) | copy-start | bytes 6291460
  163.8 1.2 copy-start.2
  163.9 188.4 %reduce-scatter.3.cloned.1.call-start = ((), (), s32[]{:S(2)}) async-start(), calls=%async_computation.3 | async-start | bytes 5242880 | tf_op jit(solution)/shard_map/reduce_scatter | solution.py:195
  170.9 2.5 copy-start.14
  175.6 2.9 copy-start.9
  178.7 47.9 %copy-start.5 = (f32[1024,2,128]{0,2,1:T(8,128)S(1)}, f32[1024,2,128]{0,2,1:T(8,128)}, u32[]{:S(2)}) copy-start(f32[1024,2,128]{0,2,1:T(8,128)} %reverse.3) | copy-start | bytes 3145732
  229.1 6.0 %copy-start.13 = (f32[32,8,8,128]{3,1,2,0:T(8,128)S(1)}, f32[32,8,8,128]{3,1,2,0:T(8,128)}, u32[]{:S(2)}) copy-start(f32[32,8,8,128]{3,1,2,0:T(8,128)} %get-tuple-element.459) | copy-start | bytes 3145732
  235.9 1.2 copy-start.12
  236.4 4.5 %copy-start.7 = (f32[8,128,2,128]{3,0,1,2:T(8,128)}, f32[8,128,2,128]{3,0,1,2:T(8,128)S(1)}, u32[]{:S(2)}) copy-start(f32[8,128,2,128]{3,0,1,2:T(8,128)S(1)} %fusion.31) | copy-start | bytes 3145732
  237.2 3.7 %copy-start.11 = (f32[32,8,8,128]{3,1,2,0:T(8,128)S(1)}, f32[32,8,8,128]{3,1,2,0:T(8,128)}, u32[]{:S(2)}) copy-start(f32[32,8,8,128]{3,1,2,0:T(8,128)} %get-tuple-element.463) | copy-start | bytes 3145732
  240.9 3.8 %slice-start = ((f32[8,128,2,128]{3,0,1,2:T(8,128)}), f32[8,1,2,128]{3,0,1,2:T(8,128)S(1)}, s32[]{:S(2)}) async-start(f32[8,128,2,128]{3,0,1,2:T(8,128)} %copy-done.7), calls=%async_computation.5 | async-start | bytes 16384 | tf_op jit(solution)/shard_map/slice | solution.py:67
  240.9 3.8 %copy-start.8 = (f32[8,128,2,128]{3,0,1,2:T(8,128)S(1)}, f32[8,128,2,128]{3,0,1,2:T(8,128)}, u32[]{:S(2)}) copy-start(f32[8,128,2,128]{3,0,1,2:T(8,128)} %copy-done.7) | copy-start | bytes 3145732
  270.3 1.4 copy-start.10
  271.9 25.7 %copy-start.4 = (f32[1024,256]{0,1:T(8,128)S(1)}, f32[1024,256]{0,1:T(8,128)}, u32[]{:S(2)}) copy-start(f32[1024,256]{0,1:T(8,128)} %copy-done.3) | copy-start | bytes 3145732
  297.7 3.1 copy-start.20
  300.7 1.2 copy-start.15
  305.2 23.3 %copy-start.19 = (f32[128,2]{0,1:T(2,128)S(1)}, f32[128,2]{0,1:T(2,128)}, u32[]{:S(2)}) copy-start(f32[128,2]{0,1:T(2,128)} %param.32) | copy-start | bytes 3076
  306.3 13.9 %collective-permute-start = (bf16[1,96,2048]{2,1,0:T(8,128)(2,1)S(1)}, bf16[1,96,2048]{2,1,0:T(8,128)(2,1)S(1)}, u32[]{:S(2)}, u32[]{:S(2)}) collective-permute-start(bf16[1,96,2048]{2,1,0:T(8,128)(2,1)S(1)} %constant_dynamic-slice_fusion.4), channel_id=1, source_target_pairs={{0,4},{4,8},{8,12},{12,0},{1,5},{5,9},{9,13},{13,1},{2,6},{6,10},{... | collective-permute-start | bytes 1179656 | tf_op jit(solution)/shard_map/ppermute | solution.py:219
  322.2 15.9 %collective-permute-start.1 = (bf16[1,96,2048]{2,1,0:T(8,128)(2,1)S(1)}, bf16[1,96,2048]{2,1,0:T(8,128)(2,1)S(1)}, u32[]{:S(2)}, u32[]{:S(2)}) collective-permute-start(bf16[1,96,2048]{2,1,0:T(8,128)(2,1)S(1)} %get-tuple-element.447), channel_id=1, source_target_pairs={{0,8},{4,12},{8,0},{12,4},{1,9},{5,13},{9,1},{13,5},{2,10},{6,14},... | collective-permute-start | bytes 1179656 | tf_op jit(solution)/shard_map/ppermute | solution.py:219
  328.1 11.5 %collective-permute-start.2 = (bf16[1,96,2048]{2,1,0:T(8,128)(2,1)S(1)}, bf16[1,96,2048]{2,1,0:T(8,128)(2,1)S(1)}, u32[]{:S(2)}, u32[]{:S(2)}) collective-permute-start(bf16[1,96,2048]{2,1,0:T(8,128)(2,1)S(1)} %get-tuple-element.446), channel_id=1, source_target_pairs={{0,12},{4,0},{8,4},{12,8},{1,13},{5,1},{9,5},{13,9},{2,14},{6,2},{... | collective-permute-start | bytes 1179656 | tf_op jit(solution)/shard_map/ppermute | solution.py:219
  344.4 7.9 %copy-start.1 = (bf16[1,512,2048]{2,1,0:T(8,128)(2,1)S(1)}, bf16[1,512,2048]{2,1,0:T(8,128)(2,1)}, u32[]{:S(2)}) copy-start(bf16[1,512,2048]{2,1,0:T(8,128)(2,1)} %param.35) | copy-start | bytes 6291460
Sparse Core Ops, SparseCore 0:
  164.0 82.2 reduce-scatter.4
  305.4 43.8 reduce-scatter.2
